TPU v7x, 32 devices: a whole 2x2x4 slice. The times are simulated.
32 devices in a mesh: fs: 8 (over z, x), tp: 4 (over y, core).
Axes of the slice: x: 2, y: 2, z: 4, core: 2. Of those that a mesh axis runs over, the one named last changes fastest.
Arguments:
- tokens: bfloat16 [4096, 2048], P('fs', 'tp'), may hold values from -16 to 16
- pre_mix_gain: bfloat16 [2048], P('tp'), may hold values from 0.099609375 to 1.8984375
- w_gate_in: bfloat16 [2048, 2048], P('fs', 'tp'), may hold values from -0.125 to 0.125
- w_input: bfloat16 [2048, 2048], P('fs', 'tp'), may hold values from -0.125 to 0.125
- mix_kernel: bfloat16 [4, 2048], P(None, 'tp'), may hold values from -3 to 3
- w_recur: bfloat16 [8, 256, 256], P('tp'), may hold values from -0.375 to 0.375
- w_inject: bfloat16 [8, 256, 256], P('tp'), may hold values from -0.375 to 0.375
- decay_param: float32 [2048], P('tp'), may hold values from 3 to 13
- w_mix_out: bfloat16 [2048, 2048], P('tp', 'fs'), may hold values from -0.125 to 0.125
- post_mix_gain: bfloat16 [2048], P('tp'), may hold values from 0.099609375 to 1.8984375
- pre_ffn_gain: bfloat16 [2048], P('tp'), may hold values from 0.099609375 to 1.8984375
- w_up_gate: bfloat16 [2048, 5632], P('fs', 'tp'), may hold values from -0.125 to 0.125
- w_up_value: bfloat16 [2048, 5632], P('fs', 'tp'), may hold values from -0.125 to 0.125
- gate_kernel: bfloat16 [3, 5632], P(None, 'tp'), may hold values from -3 to 3
- value_kernel: bfloat16 [3, 5632], P(None, 'tp'), may hold values from -3 to 3
- w_down: bfloat16 [5632, 2048], P('tp', 'fs'), may hold values from -0.078125 to 0.078125
- post_ffn_gain: bfloat16 [2048], P('tp'), may hold values from 0.099609375 to 1.8984375
Outputs:
- layer_out: bfloat16 [4096, 2048], P('fs', 'tp')
All inputs are finite; a program needn't handle non-finite values.
Results may differ from a plain program's by a relative error of at most 0.015.
Values may be sent and summed in bfloat16 or wider, within the bound.
A program may use at most 64 MiB of HBM per device.

v0:
```python
import jax
import jax.numpy as jnp
from jax import lax
from jax.sharding import PartitionSpec as P

D = 2048
norm_eps = 1e-06
gate_power = 8.0


def row_normed(values, row_gain):
    widened = values.astype(jnp.float32)
    squares = lax.psum(jnp.sum(widened * widened, axis=1), "tp")
    factor = lax.rsqrt(squares / D + norm_eps)
    return widened * factor[:, None] * row_gain.astype(jnp.float32)[None, :]


def gathered_rows(values, row_gain):
    return lax.all_gather(
        row_normed(values, row_gain).astype(jnp.bfloat16), "tp", axis=1, tiled=True
    )


def summed_terms(partial_value):
    return lax.psum_scatter(
        partial_value.astype(jnp.bfloat16), "tp", scatter_dimension=1, tiled=True
    ).astype(jnp.float32)


def causal_conv(values, kernel):
    length = values.shape[0]
    widths = kernel.shape[0]
    padded = jnp.pad(values.astype(jnp.float32), ((widths - 1, 0), (0, 0)))
    weights = kernel.astype(jnp.float32)
    result = padded[0:length] * weights[0]
    for offset in range(1, widths):
        result = result + padded[offset : offset + length] * weights[offset]
    return result


def pair_folder(inputs, pieces):
    return (
        jnp.dot(inputs, pieces[0], preferred_element_type=jnp.float32),
        jnp.dot(inputs, pieces[1], preferred_element_type=jnp.float32),
    )


def linear_combine(earlier, latter):
    return (earlier[0] * latter[0], latter[0] * earlier[1] + latter[1])


def shards(
    tokens,
    pre_mix_gain,
    w_gate_in,
    w_input,
    mix_kernel,
    w_recur,
    w_inject,
    decay_param,
    w_mix_out,
    post_mix_gain,
    pre_ffn_gain,
    w_up_gate,
    w_up_value,
    gate_kernel,
    value_kernel,
    w_down,
    post_ffn_gain,
):
    normed_in = gathered_rows(tokens, pre_mix_gain)
    length = normed_in.shape[0]
    gate_sum, input_sum = pair_folder(
        normed_in,
        (
            lax.all_gather(w_gate_in, "fs", axis=0, tiled=True),
            lax.all_gather(w_input, "fs", axis=0, tiled=True),
        ),
    )
    gate_rows = gate_sum.astype(jnp.bfloat16)
    input_rows = input_sum.astype(jnp.bfloat16)
    smoothed = causal_conv(input_rows, mix_kernel).astype(jnp.bfloat16)
    by_head = smoothed.reshape(length, w_recur.shape[0], w_recur.shape[1])
    recur_gate = jax.nn.sigmoid(
        jnp.einsum("thi,hij->thj", by_head, w_recur, preferred_element_type=jnp.float32)
    ).reshape(length, -1)
    inject_gate = jax.nn.sigmoid(
        jnp.einsum("thi,hij->thj", by_head, w_inject, preferred_element_type=jnp.float32)
    ).reshape(length, -1)
    log_retain = -gate_power * recur_gate * jax.nn.softplus(-decay_param)[None, :]
    retain = jnp.exp(log_retain)
    driven = jnp.sqrt(-jnp.expm1(2.0 * log_retain)) * inject_gate * smoothed.astype(jnp.float32)
    _, states = lax.associative_scan(linear_combine, (retain, driven), axis=0)
    hidden = (jax.nn.gelu(gate_rows.astype(jnp.float32), approximate=True) * states).astype(
        jnp.bfloat16
    )
    mixer_terms = jnp.dot(
        hidden,
        lax.all_gather(w_mix_out, "fs", axis=1, tiled=True),
        preferred_element_type=jnp.float32,
    )
    middle = (
        tokens.astype(jnp.float32) + row_normed(summed_terms(mixer_terms), post_mix_gain)
    ).astype(jnp.bfloat16)
    normed_mid = gathered_rows(middle, pre_ffn_gain)
    up_gate, up_value = pair_folder(
        normed_mid,
        (
            lax.all_gather(w_up_gate, "fs", axis=0, tiled=True),
            lax.all_gather(w_up_value, "fs", axis=0, tiled=True),
        ),
    )
    conv_gate_out = causal_conv(up_gate.astype(jnp.bfloat16), gate_kernel)
    conv_value_out = causal_conv(up_value.astype(jnp.bfloat16), value_kernel)
    activated = (jax.nn.gelu(conv_gate_out, approximate=True) * conv_value_out).astype(jnp.bfloat16)
    ffn_terms = jnp.dot(
        activated,
        lax.all_gather(w_down, "fs", axis=1, tiled=True),
        preferred_element_type=jnp.float32,
    )
    return (middle.astype(jnp.float32) + row_normed(summed_terms(ffn_terms), post_ffn_gain)).astype(
        jnp.bfloat16
    )


def solution(mesh):
    return jax.shard_map(
        shards,
        mesh=mesh,
        in_specs=(
            P("fs", "tp"),
            P("tp"),
            P("fs", "tp"),
            P("fs", "tp"),
            P(None, "tp"),
            P("tp", None, None),
            P("tp", None, None),
            P("tp"),
            P("tp", "fs"),
            P("tp"),
            P("tp"),
            P("fs", "tp"),
            P("fs", "tp"),
            P(None, "tp"),
            P(None, "tp"),
            P("tp", "fs"),
            P("tp"),
        ),
        out_specs=P("fs", "tp"),
        check_vma=False,
    )
```

profile of v0, /device:TPU:0, one launch (start us, length us, event | category | flops | bytes accessed | tf_op | source)
XLA Modules:
  0.0 595.2 jit_solution(16134172578060432192)
XLA Ops:
  7.8 8.4 %psum.28 = f32[512]{0:T(512)S(1)} all-reduce(f32[512]{0:T(512)S(1)} %fusion.33), channel_id=1, replica_groups=mesh['fs'=8,'tp'=4] {'tp'}, use_global_device_ids=true, to_apply=%region_1.0 | all-reduce | flops 512 | bytes 4096 | tf_op jit(solution)/shard_map/psum | solution.py:13
  16.9 2.0 fusion.35
  21.1 20.8 %all-gather.9.cloned.1.call-done = bf16[512,2048]{1,0:T(8,128)(2,1)} async-done(((bf16[512,512]{1,0:T(8,128)(2,1)}), bf16[512,2048]{1,0:T(8,128)(2,1)}) %all-gather.9.cloned.1.call-update) | async-done | bytes 2097168 | tf_op jit(solution)/shard_map/all_gather | solution.py:19
  42.0 51.2 %all-gather.13.cloned.1.call-done = bf16[2048,512]{1,0:T(8,128)(2,1)} async-done(((bf16[256,512]{1,0:T(8,128)(2,1)}), bf16[2048,512]{1,0:T(8,128)(2,1)}) %all-gather.13.cloned.1.call-update) | async-done | bytes 2097168 | tf_op jit(solution)/shard_map/all_gather | solution.py:77
  93.2 3.5 fusion.28
  97.7 1.3 copy.26
  99.5 1.4 copy.27
  100.9 2.8 multiply_exponential_fusion
  103.7 2.1 slice.271
  105.8 2.1 slice.272
  107.8 2.1 slice.270
  109.9 2.1 slice.274
  112.0 1.7 fusion.78
  113.7 1.4 slice.277
  115.1 1.4 slice.278
  116.5 1.4 slice.276
  117.8 1.4 slice.280
  119.2 2.0 fusion.79
  122.6 1.6 slice.282
  124.2 1.6 slice.286
  125.8 1.8 fusion.80
  128.8 1.5 slice.288
  130.3 1.5 slice.292
  131.9 1.6 fusion.81
  133.4 1.4 slice.295
  134.9 1.4 slice.296
  136.3 1.4 slice.294
  137.8 1.4 slice.298
  139.2 1.4 fusion.82
  140.7 1.4 slice.301
  142.0 1.4 slice.302
  143.4 1.4 slice.300
  144.8 1.4 slice.304
  146.1 1.4 fusion.83
  148.7 1.3 slice.306
  150.0 1.3 slice.310
  151.3 1.4 fusion.85
  152.7 1.3 slice.313
  155.3 1.3 slice.312
  157.9 1.3 slice.305
  161.2 1.4 slice.324
  162.5 1.3 slice.354
  163.8 1.4 slice.293
  165.3 1.5 slice.326
  168.0 1.5 slice.287
  173.3 1.4 slice.275
  174.7 1.4 slice.332
  184.8 2.8 pad.84
  188.1 5.7 all-gather.15.cloned.1.call-done
  193.8 7.2 %convolution_convert_fusion.2 = bf16[512,2048]{1,0:T(8,128)(2,1)} fusion(bf16[512,2048]{1,0:T(8,128)(2,1)} %all-gather.15.cloned.1.call-done, bf16[512,2048]{1,0:T(8,128)(2,1)} %all-gather.9.cloned.1.call-done, bf16[2048,512]{1,0:T(8,128)(2,1)} %all-gather.11.cloned.1.call-done, f32[512,512]{1,0:T(8,128)S(1)} %pad.83, f32[512,512]{1,0:T(8,128)} %pad.84), kind=kOutput, calls=%fused_computation.5 | convolution fusion | flops 2151940096 | bytes 10485760 | tf_op jit(solution)/shard_map/dot_general | solution.py:97
  201.7 28.8 %reduce-scatter.3.cloned.1.call-done = bf16[512,512]{1,0:T(8,128)(2,1)} async-done(((bf16[512,2048]{1,0:T(8,128)(2,1)}), bf16[512,512]{1,0:T(8,128)(2,1)}) %reduce-scatter.3.cloned.1.call-update) | async-done | bytes 524304 | tf_op jit(solution)/shard_map/reduce_scatter | solution.py:25
  231.7 5.8 psum.29
  237.5 1.5 fusion.37
  239.0 5.7 psum.30
  247.3 77.5 %all-gather.21.cloned.1.call-done = bf16[2048,1408]{1,0:T(8,128)(2,1)} async-done(((bf16[256,1408]{1,0:T(8,128)(2,1)}), bf16[2048,1408]{1,0:T(8,128)(2,1)}) %all-gather.21.cloned.1.call-update) | async-done | bytes 5767184 | tf_op jit(solution)/shard_map/all_gather | solution.py:110
  324.9 22.3 %all-gather.17.cloned.1.call-done = bf16[512,2048]{1,0:T(8,128)(2,1)} async-done(((bf16[512,512]{1,0:T(8,128)(2,1)}), bf16[512,2048]{1,0:T(8,128)(2,1)}) %all-gather.17.cloned.1.call-update) | async-done | bytes 2097168 | tf_op jit(solution)/shard_map/all_gather | solution.py:19
  347.2 8.4 %fusion = f32[512,1408]{1,0:T(8,128)} fusion(bf16[512,2048]{1,0:T(8,128)(2,1)} %all-gather.17.cloned.1.call-done, bf16[2048,1408]{1,0:T(8,128)(2,1)} %all-gather.21.cloned.1.call-done), kind=kOutput, calls=%fused_computation.2 | convolution fusion | flops 2954231808 | bytes 10747904 | tf_op jit(solution)/shard_map/dot_general | solution.py:44
  355.6 86.1 %all-gather.19.cloned.1.call-done = bf16[2048,1408]{1,0:T(8,128)(2,1)} async-done(((bf16[256,1408]{1,0:T(8,128)(2,1)}), bf16[2048,1408]{1,0:T(8,128)(2,1)}) %all-gather.19.cloned.1.call-update) | async-done | bytes 5767184 | tf_op jit(solution)/shard_map/all_gather | solution.py:109
  441.8 7.6 %fusion.1 = f32[512,1408]{1,0:T(8,128)} fusion(bf16[512,2048]{1,0:T(8,128)(2,1)S(1)} %copy-done.26, bf16[2048,1408]{1,0:T(8,128)(2,1)} %all-gather.19.cloned.1.call-done), kind=kOutput, calls=%fused_computation.4 | convolution fusion | flops 2954231808 | bytes 10747904 | tf_op jit(solution)/shard_map/dot_general | solution.py:43
  449.4 85.8 %all-gather.23.cloned.1.call-done = bf16[1408,2048]{1,0:T(8,128)(2,1)} async-done(((bf16[1408,256]{1,0:T(8,128)(2,1)}), bf16[1408,2048]{1,0:T(8,128)(2,1)}) %all-gather.23.cloned.1.call-update) | async-done | bytes 5767184 | tf_op jit(solution)/shard_map/all_gather | solution.py:118
  535.2 14.5 %convolution_convert_fusion.3 = bf16[512,2048]{1,0:T(8,128)(2,1)} fusion(bf16[1408,2048]{1,0:T(8,128)(2,1)} %all-gather.23.cloned.1.call-done, f32[512,1408]{1,0:T(8,128)} %fusion, f32[512,1408]{1,0:T(8,128)} %fusion.1, f32[1408]{0:T(1024)S(1)} %get-tuple-element.9, f32[1408]{0:T(1024)S(1)} %get-tuple-element.10, f32[1408]{0:T(1024)S(1)} %get-tuple-element.8, ...), kind=kOutput, calls=%fused_computation.6 | convolution fusion | flops 2968256512 | bytes 13665280 | tf_op jit(solution)/shard_map/dot_general | solution.py:116
  549.7 29.5 %reduce-scatter.5.cloned.1.call-done = bf16[512,512]{1,0:T(8,128)(2,1)} async-done(((bf16[512,2048]{1,0:T(8,128)(2,1)}), bf16[512,512]{1,0:T(8,128)(2,1)}) %reduce-scatter.5.cloned.1.call-update) | async-done | bytes 524304 | tf_op jit(solution)/shard_map/reduce_scatter | solution.py:25
  580.5 5.8 psum.31
  586.2 2.1 fusion.40
  (159 shorter events, 33.4 us)
Async XLA Ops:
  6.5 90.6 %copy-start = (bf16[2,256,256]{2,1,0:T(8,128)(2,1)S(1)}, bf16[2,256,256]{2,1,0:T(8,128)(2,1)}, u32[]{:S(2)}) copy-start(bf16[2,256,256]{2,1,0:T(8,128)(2,1)} %param.22) | copy-start | bytes 786436
  6.5 14.5 %copy-start.12 = (bf16[4,512]{1,0:T(4,128)(2,1)S(1)}, bf16[4,512]{1,0:T(4,128)(2,1)}, u32[]{:S(2)}) copy-start(bf16[4,512]{1,0:T(4,128)(2,1)} %param.21) | copy-start | bytes 12292
  6.5 14.5 %copy-start.22 = (f32[512]{0:T(512)S(1)}, f32[512]{0:T(512)}, u32[]{:S(2)}) copy-start(f32[512]{0:T(512)} %param.24) | copy-start | bytes 6148
  6.5 35.4 %all-gather.9.cloned.1.call-start = ((), (), s32[]{:S(2)}) async-start(), calls=%async_computation.2 | async-start | bytes 2621440 | tf_op jit(solution)/shard_map/all_gather | solution.py:19
  18.9 74.3 %all-gather.13.cloned.1.call-start = ((), (), s32[]{:S(2)}) async-start(), calls=%async_computation.4 | async-start | bytes 2359296 | tf_op jit(solution)/shard_map/all_gather | solution.py:77
  19.7 168.4 %all-gather.11.cloned.1.call-start = ((), (), s32[]{:S(2)}) async-start(), calls=%async_computation.3 | async-start | bytes 2359296 | tf_op jit(solution)/shard_map/all_gather | solution.py:76
  20.4 173.4 %all-gather.15.cloned.1.call-start = ((), (), s32[]{:S(2)}) async-start(), calls=%async_computation.5 | async-start | bytes 2359296 | tf_op jit(solution)/shard_map/all_gather | solution.py:99
  21.0 209.5 %reduce-scatter.3.cloned.1.call-start = ((), (), s32[]{:S(2)}) async-start(), calls=%async_computation.6 | async-start | bytes 2621440 | tf_op jit(solution)/shard_map/reduce_scatter | solution.py:25
  97.2 1.8 copy-start.27
  173.2 5.2 copy-start.11
  173.2 5.2 copy-start.13
  173.2 5.2 copy-start.14
  173.2 5.2 copy-start.17
  173.2 5.2 copy-start.8
  173.2 6.0 %copy-start.9 = (f32[3,512]{1,0:T(4,128)S(1)}, f32[3,512]{1,0:T(4,128)}, u32[]{:S(2)}) copy-start(f32[3,512]{1,0:T(4,128)} %slice.305) | copy-start | bytes 18436
  173.2 6.0 %copy-start.10 = (f32[3,512]{1,0:T(4,128)S(1)}, f32[3,512]{1,0:T(4,128)}, u32[]{:S(2)}) copy-start(f32[3,512]{1,0:T(4,128)} %slice.322) | copy-start | bytes 18436
  173.3 6.1 %copy-start.21 = (f32[1,512]{1,0:T(1,128)S(1)}, f32[1,512]{1,0:T(1,128)}, u32[]{:S(2)}) copy-start(f32[1,512]{1,0:T(1,128)} %slice.355) | copy-start | bytes 6148
  173.3 6.1 %copy-start.7 = (f32[7,512]{1,0:T(8,128)S(1)}, f32[7,512]{1,0:T(8,128)}, u32[]{:S(2)}) copy-start(f32[7,512]{1,0:T(8,128)} %slice.324) | copy-start | bytes 43012
  173.3 6.1 %copy-start.20 = (f32[1,512]{1,0:T(1,128)S(1)}, f32[1,512]{1,0:T(1,128)}, u32[]{:S(2)}) copy-start(f32[1,512]{1,0:T(1,128)} %slice.354) | copy-start | bytes 6148
  173.3 6.2 %copy-start.6 = (f32[15,512]{1,0:T(8,128)S(1)}, f32[15,512]{1,0:T(8,128)}, u32[]{:S(2)}) copy-start(f32[15,512]{1,0:T(8,128)} %slice.293) | copy-start | bytes 92164
  173.3 7.7 %copy-start.5 = (f32[31,512]{1,0:T(8,128)S(1)}, f32[31,512]{1,0:T(8,128)}, u32[]{:S(2)}) copy-start(f32[31,512]{1,0:T(8,128)} %slice.287) | copy-start | bytes 190468
  177.8 6.6 %copy-start.3 = (f32[127,512]{1,0:T(8,128)S(1)}, f32[127,512]{1,0:T(8,128)}, u32[]{:S(2)}) copy-start(f32[127,512]{1,0:T(8,128)} %slice.275) | copy-start | bytes 780292
  177.8 6.6 %copy-start.4 = (f32[127,512]{1,0:T(8,128)S(1)}, f32[127,512]{1,0:T(8,128)}, u32[]{:S(2)}) copy-start(f32[127,512]{1,0:T(8,128)} %slice.332) | copy-start | bytes 780292
  179.5 5.1 copy-start.19
  184.7 3.2 copy-start.18
  188.1 13.6 %copy-start.23 = (bf16[512]{0:T(512)(128)(2,1)S(1)}, bf16[512]{0:T(512)(128)(2,1)}, u32[]{:S(2)}) copy-start(bf16[512]{0:T(512)(128)(2,1)} %param.26) | copy-start | bytes 3076
  188.1 13.6 %copy-start.24 = (bf16[512]{0:T(512)(128)(2,1)S(1)}, bf16[512]{0:T(512)(128)(2,1)}, u32[]{:S(2)}) copy-start(bf16[512]{0:T(512)(128)(2,1)} %param.27) | copy-start | bytes 3076
  201.0 36.5 %copy-start.2 = (bf16[512,512]{1,0:T(8,128)(2,1)S(1)}, bf16[512,512]{1,0:T(8,128)(2,1)}, u32[]{:S(2)}) copy-start(bf16[512,512]{1,0:T(8,128)(2,1)} %param.17) | copy-start | bytes 1572868
  201.0 46.2 %copy-start.15 = (bf16[3,1408]{1,0:T(4,128)(2,1)S(1)}, bf16[3,1408]{1,0:T(4,128)(2,1)}, u32[]{:S(2)}) copy-start(bf16[3,1408]{1,0:T(4,128)(2,1)} %param.30) | copy-start | bytes 25348
  201.0 46.2 %copy-start.16 = (bf16[3,1408]{1,0:T(4,128)(2,1)S(1)}, bf16[3,1408]{1,0:T(4,128)(2,1)}, u32[]{:S(2)}) copy-start(bf16[3,1408]{1,0:T(4,128)(2,1)} %param.31) | copy-start | bytes 25348
  201.0 123.9 %all-gather.21.cloned.1.call-start = ((), (), s32[]{:S(2)}) async-start(), calls=%async_computation.9 | async-start | bytes 6488064 | tf_op jit(solution)/shard_map/all_gather | solution.py:110
  201.6 145.6 %all-gather.17.cloned.1.call-start = ((), (), s32[]{:S(2)}) async-start(), calls=%async_computation.7 | async-start | bytes 2621440 | tf_op jit(solution)/shard_map/all_gather | solution.py:19
  245.7 196.1 %all-gather.19.cloned.1.call-start = ((), (), s32[]{:S(2)}) async-start(), calls=%async_computation.8 | async-start | bytes 6488064 | tf_op jit(solution)/shard_map/all_gather | solution.py:109
  246.4 288.7 %all-gather.23.cloned.1.call-start = ((), (), s32[]{:S(2)}) async-start(), calls=%async_computation.10 | async-start | bytes 6488064 | tf_op jit(solution)/shard_map/all_gather | solution.py:118
  247.1 332.1 %reduce-scatter.5.cloned.1.call-start = ((), (), s32[]{:S(2)}) async-start(), calls=%async_computation.11 | async-start | bytes 2621440 | tf_op jit(solution)/shard_map/reduce_scatter | solution.py:25
  347.2 94.5 %copy-start.26 = (bf16[512,2048]{1,0:T(8,128)(2,1)S(1)}, bf16[512,2048]{1,0:T(8,128)(2,1)}, u32[]{:S(2)}) copy-start(bf16[512,2048]{1,0:T(8,128)(2,1)} %all-gather.17.cloned.1.call-done) | copy-start | bytes 6291460
  535.1 14.6 %copy-start.25 = (bf16[512]{0:T(512)(128)(2,1)S(1)}, bf16[512]{0:T(512)(128)(2,1)}, u32[]{:S(2)}) copy-start(bf16[512]{0:T(512)(128)(2,1)} %param.33) | copy-start | bytes 3076
  535.2 53.2 %copy-start.1 = (bf16[2,256,256]{2,1,0:T(8,128)(2,1)S(1)}, bf16[2,256,256]{2,1,0:T(8,128)(2,1)}, u32[]{:S(2)}) copy-start(bf16[2,256,256]{2,1,0:T(8,128)(2,1)} %param.22) | copy-start | bytes 786436
Sparse Core Ops, SparseCore 0:
  19.1 22.8 all-gather.8
  44.1 49.0 all-gather.12
  95.3 47.6 all-gather.10
  144.9 48.8 all-gather.14
  201.1 29.3 reduce-scatter.2
  232.5 92.2 all-gather.20
  326.4 20.7 all-gather.16
  349.4 92.2 all-gather.18
  443.8 91.3 all-gather.22
  549.8 29.3 reduce-scatter.4
where the time goes:
time: 597 us; the launch traced here: 595 us
  waiting for transfers between devices  412 us (69%)
  local copies, waits for them, and re-layouts  69.6 us (12%)
  matrix products  42.1 us (7%)
  other arithmetic  31.5 us (5%)
  blocking collectives  25.6 us (4%)
  between operations  14.2 us (2%)
    all_gather x1, waiting for transfers between devices, shards(): lax.all_gather(w_up_gate, 'fs', axis=0, tiled=True)  86.1 us
    all_gather x1, waiting for transfers between devices, shards(): lax.all_gather(w_down, 'fs', axis=1, tiled=True)  85.8 us
    all_gather x1, waiting for transfers between devices, shards(): lax.all_gather(w_up_value, 'fs', axis=0, tiled=True)  77.5 us
    slice x53, local copies, waits for them, and re-layouts, shards(): _, states = lax.associative_scan(linear_combine, (retain, driven), axis=0)  63.3 us
    reduce_scatter x2, waiting for transfers between devices, summed_terms(): lax.psum_scatter(partial_value.astype(jnp.bfloat16), 'tp', scatter_dimens...  58.3 us
    all_gather x1, waiting for transfers between devices, shards(): lax.all_gather(w_input, 'fs', axis=0, tiled=True)  51.2 us
    all_gather x2, waiting for transfers between devices, gathered_rows(): lax.all_gather(row_normed(values, row_gain).astype(jnp.bfloat16), 'tp', a...  43.2 us
    psum x4, blocking collectives, row_normed(): squares = lax.psum(jnp.sum(widened * widened, axis=1), 'tp')  25.6 us
  transfers between devices with their start and end apart: 10, of which 9 were waited for; matrix products, arithmetic and copies ran while one was open for 19% of the time, Pallas kernels for 0%

commit v1 on v0

--- a/solution.py
+++ b/solution.py
@@ -16,8 +16,14 @@
 
 
 def gathered_rows(values, row_gain):
-    return lax.all_gather(
-        row_normed(values, row_gain).astype(jnp.bfloat16), "tp", axis=1, tiled=True
+    return jnp.concatenate(
+        lax.all_to_all(
+            jnp.stack([row_normed(values, row_gain).astype(jnp.bfloat16)] * lax.axis_size("tp")),
+            "tp",
+            0,
+            0,
+        ),
+        axis=1,
     )
 
 

time: 597 us -> 542 us (0.908)
  waiting for transfers between devices: 412 us -> 348 us
  starting transfers between devices: 0.54 us -> 7.62 us
    all_to_all x0 -> x2, waiting for transfers between devices: none -> 50.2 us  [gathered_rows(): lax.all_to_all(jnp.stack([row_normed(values, row_gain).astype(jnp.bfloat1...]
    all_gather x2 -> x0, waiting for transfers between devices: 43.2 us -> none  [gathered_rows(): lax.all_gather(row_normed(values, row_gain).astype(jnp.bfloat16), 'tp', a...]
    all_gather x1, waiting for transfers between devices: 51.2 us -> 10.6 us  [shards(): lax.all_gather(w_input, 'fs', axis=0, tiled=True)]
    all_gather x1, waiting for transfers between devices: 77.5 us -> 48.9 us  [shards(): lax.all_gather(w_up_value, 'fs', axis=0, tiled=True)]
    all_to_all x0 -> x2, starting transfers between devices: none -> 7.34 us  [gathered_rows(): lax.all_to_all(jnp.stack([row_normed(values, row_gain).astype(jnp.bfloat1...]
    all_gather x1, waiting for transfers between devices: 0.02 us -> 6.13 us  [shards(): lax.all_gather(w_gate_in, 'fs', axis=0, tiled=True)]
  transfers between devices with their start and end apart: 10 -> 10, of which waited for: 9 -> 9; matrix products, arithmetic and copies ran while one was open for 19% -> 22% of each run, Pallas kernels for 0% -> 0%
where the time goes in v1:
time: 542 us; the launch traced here: 539 us
  waiting for transfers between devices  348 us (64%)
  local copies, waits for them, and re-layouts  73 us (13%)
  matrix products  41 us (8%)
  other arithmetic  29.9 us (6%)
  blocking collectives  25.8 us (5%)
  between operations  14.2 us (3%)
  starting transfers between devices  7.62 us (1%)
    all_gather x1, waiting for transfers between devices, shards(): lax.all_gather(w_down, 'fs', axis=1, tiled=True)  85.6 us
    all_gather x1, waiting for transfers between devices, shards(): lax.all_gather(w_up_gate, 'fs', axis=0, tiled=True)  84.9 us
    slice x53, local copies, waits for them, and re-layouts, shards(): _, states = lax.associative_scan(linear_combine, (retain, driven), axis=0)  63.4 us
    reduce_scatter x2, waiting for transfers between devices, summed_terms(): lax.psum_scatter(partial_value.astype(jnp.bfloat16), 'tp', scatter_dimens...  57.4 us
    all_to_all x2, waiting for transfers between devices, gathered_rows(): lax.all_to_all(jnp.stack([row_normed(values, row_gain).astype(jnp.bfloat1...  50.2 us
    all_gather x1, waiting for transfers between devices, shards(): lax.all_gather(w_up_value, 'fs', axis=0, tiled=True)  48.9 us
    psum x4, blocking collectives, row_normed(): squares = lax.psum(jnp.sum(widened * widened, axis=1), 'tp')  25.8 us
    dot_general x1, matrix products, shards(): jnp.dot(activated, lax.all_gather(w_down, 'fs', axis=1, tiled=True), pref...  14.7 us
  transfers between devices with their start and end apart: 10, of which 9 were waited for; matrix products, arithmetic and copies ran while one was open for 22% of the time, Pallas kernels for 0%

profile of v1, /device:TPU:0, one launch (start us, length us, event | category | flops | bytes accessed | tf_op | source)
XLA Modules:
  0.0 539.2 jit_solution(3861532676276726477)
XLA Ops:
  9.9 8.4 %psum.28 = f32[512]{0:T(512)S(1)} all-reduce(f32[512]{0:T(512)S(1)} %fusion.33), channel_id=1, replica_groups=mesh['fs'=8,'tp'=4] {'tp'}, use_global_device_ids=true, to_apply=%region_1.0 | all-reduce | flops 512 | bytes 4096 | tf_op jit(solution)/shard_map/psum | solution.py:13
  19.8 1.5 stack.4
  21.3 3.7 all-to-all-start
  25.9 24.8 %all-to-all-done = bf16[4,512,512]{1,2,0:T(8,128)(2,1)S(1)} async-done(((bf16[4,512,512]{1,2,0:T(8,128)(2,1)}), bf16[4,512,512]{1,2,0:T(8,128)(2,1)S(1)}, u32[]{:S(2)}, u32[]{:S(2)}) %all-to-all-start) | async-done | bytes 2097184 | tf_op jit(solution)/shard_map/all_to_all | solution.py:20
  50.7 10.6 %all-gather.9.cloned.1.call-done = bf16[2048,512]{1,0:T(8,128)(2,1)} async-done(((bf16[256,512]{1,0:T(8,128)(2,1)}), bf16[2048,512]{1,0:T(8,128)(2,1)}) %all-gather.9.cloned.1.call-update) | async-done | bytes 2097168 | tf_op jit(solution)/shard_map/all_gather | solution.py:83
  61.3 2.9 fusion.28
  65.2 1.3 copy.34
  67.0 1.4 copy.35
  68.4 2.8 multiply_exponential_fusion
  71.2 2.1 slice.271
  73.3 2.1 slice.272
  75.3 2.1 slice.270
  77.4 2.1 slice.274
  79.5 1.7 fusion.78
  81.2 1.4 slice.277
  82.6 1.4 slice.278
  84.0 1.4 slice.276
  85.3 1.4 slice.280
  86.7 2.0 fusion.79
  90.1 1.6 slice.282
  91.7 1.6 slice.286
  93.3 1.8 fusion.80
  96.3 1.5 slice.288
  97.9 1.5 slice.292
  99.4 1.6 fusion.81
  101.0 1.4 slice.295
  102.5 1.4 slice.296
  103.9 1.5 slice.294
  105.4 1.4 slice.298
  106.8 1.4 fusion.82
  108.2 1.4 slice.301
  109.6 1.4 slice.302
  111.0 1.4 slice.300
  112.3 1.4 slice.304
  113.7 1.4 fusion.83
  116.3 1.3 slice.306
  117.6 1.3 slice.310
  118.9 1.4 fusion.85
  125.5 1.3 slice.305
  128.7 1.4 slice.324
  131.4 1.4 slice.293
  132.8 1.4 slice.326
  135.6 1.5 slice.287
  140.9 1.4 slice.275
  142.3 1.4 slice.332
  152.4 2.7 pad.84
  155.6 6.1 %all-gather.7.cloned.1.call-done = bf16[2048,512]{1,0:T(8,128)(2,1)} async-done(((bf16[256,512]{1,0:T(8,128)(2,1)}), bf16[2048,512]{1,0:T(8,128)(2,1)}) %all-gather.7.cloned.1.call-update) | async-done | bytes 2097168 | tf_op jit(solution)/shard_map/all_gather | solution.py:82
  161.7 7.1 %convolution_convert_fusion.2 = bf16[512,2048]{1,0:T(8,128)(2,1)} fusion(bf16[512,2048]{1,0:T(8,128)(2,1)} %all-gather.11.cloned.1.call-done, bf16[512,2048]{0,1:T(8,128)(2,1)} %bitcast.35, bf16[2048,512]{1,0:T(8,128)(2,1)} %all-gather.7.cloned.1.call-done, f32[512,512]{1,0:T(8,128)S(1)} %pad.83, f32[512,512]{1,0:T(8,128)} %pad.84), kind=kOutput, calls=%fused_computation.5 | convolution fusion | flops 2151940096 | bytes 10485760 | tf_op jit(solution)/shard_map/dot_general | solution.py:103
  170.8 27.9 %reduce-scatter.3.cloned.1.call-done = bf16[512,512]{1,0:T(8,128)(2,1)} async-done(((bf16[512,2048]{1,0:T(8,128)(2,1)}), bf16[512,512]{1,0:T(8,128)(2,1)}) %reduce-scatter.3.cloned.1.call-update) | async-done | bytes 524304 | tf_op jit(solution)/shard_map/reduce_scatter | solution.py:31
  199.9 5.9 %psum.29 = f32[512]{0:T(512)S(1)} all-reduce(f32[512]{0:T(512)S(1)} %fusion.29), channel_id=1, replica_groups=mesh['fs'=8,'tp'=4] {'tp'}, use_global_device_ids=true, to_apply=%region_4.5 | all-reduce | flops 512 | bytes 4096 | tf_op jit(solution)/shard_map/psum | solution.py:13
  205.9 1.5 fusion.37
  207.4 5.7 %psum.30 = f32[512]{0:T(512)S(1)} all-reduce(f32[512]{0:T(512)S(1)} %get-tuple-element.11), channel_id=1, replica_groups=mesh['fs'=8,'tp'=4] {'tp'}, use_global_device_ids=true, to_apply=%region_6.7 | all-reduce | flops 512 | bytes 4096 | tf_op jit(solution)/shard_map/psum | solution.py:13
  213.5 1.5 stack.5
  215.0 3.6 all-to-all-start.1
  218.8 25.4 %all-to-all-done.1 = bf16[4,512,512]{1,2,0:T(8,128)(2,1)S(1)} async-done(((bf16[4,512,512]{1,2,0:T(8,128)(2,1)}), bf16[4,512,512]{1,2,0:T(8,128)(2,1)S(1)}, u32[]{:S(2)}, u32[]{:S(2)}) %all-to-all-start.1) | async-done | bytes 2097184 | tf_op jit(solution)/shard_map/all_to_all | solution.py:20
  244.2 48.9 %all-gather.15.cloned.1.call-done = bf16[2048,1408]{1,0:T(8,128)(2,1)} async-done(((bf16[256,1408]{1,0:T(8,128)(2,1)}), bf16[2048,1408]{1,0:T(8,128)(2,1)}) %all-gather.15.cloned.1.call-update) | async-done | bytes 5767184 | tf_op jit(solution)/shard_map/all_gather | solution.py:116
  293.1 7.7 %fusion = f32[512,1408]{1,0:T(8,128)} fusion(bf16[512,2048]{0,1:T(8,128)(2,1)S(1)} %bitcast.36, bf16[2048,1408]{1,0:T(8,128)(2,1)} %all-gather.15.cloned.1.call-done), kind=kOutput, calls=%fused_computation.2 | convolution fusion | flops 2954231808 | bytes 10747904 | tf_op jit(solution)/shard_map/dot_general | solution.py:50
  300.7 84.9 %all-gather.13.cloned.1.call-done = bf16[2048,1408]{1,0:T(8,128)(2,1)} async-done(((bf16[256,1408]{1,0:T(8,128)(2,1)}), bf16[2048,1408]{1,0:T(8,128)(2,1)}) %all-gather.13.cloned.1.call-update) | async-done | bytes 5767184 | tf_op jit(solution)/shard_map/all_gather | solution.py:115
  385.6 7.7 %fusion.1 = f32[512,1408]{1,0:T(8,128)} fusion(bf16[512,2048]{0,1:T(8,128)(2,1)S(1)} %bitcast.37, bf16[2048,1408]{1,0:T(8,128)(2,1)} %all-gather.13.cloned.1.call-done), kind=kOutput, calls=%fused_computation.4 | convolution fusion | flops 2954231808 | bytes 10747904 | tf_op jit(solution)/shard_map/dot_general | solution.py:49
  393.4 85.6 %all-gather.17.cloned.1.call-done = bf16[1408,2048]{1,0:T(8,128)(2,1)} async-done(((bf16[1408,256]{1,0:T(8,128)(2,1)}), bf16[1408,2048]{1,0:T(8,128)(2,1)}) %all-gather.17.cloned.1.call-update) | async-done | bytes 5767184 | tf_op jit(solution)/shard_map/all_gather | solution.py:124
  479.0 14.7 %convolution_convert_fusion.3 = bf16[512,2048]{1,0:T(8,128)(2,1)} fusion(bf16[1408,2048]{1,0:T(8,128)(2,1)} %all-gather.17.cloned.1.call-done, f32[512,1408]{1,0:T(8,128)} %fusion, f32[512,1408]{1,0:T(8,128)} %fusion.1, f32[1408]{0:T(1024)S(1)} %get-tuple-element.9, f32[1408]{0:T(1024)S(1)} %get-tuple-element.10, f32[1408]{0:T(1024)S(1)} %get-tuple-element.8, ...), kind=kOutput, calls=%fused_computation.6 | convolution fusion | flops 2968256512 | bytes 13665280 | tf_op jit(solution)/shard_map/dot_general | solution.py:122
  493.8 29.5 %reduce-scatter.5.cloned.1.call-done = bf16[512,512]{1,0:T(8,128)(2,1)} async-done(((bf16[512,2048]{1,0:T(8,128)(2,1)}), bf16[512,512]{1,0:T(8,128)(2,1)}) %reduce-scatter.5.cloned.1.call-update) | async-done | bytes 524304 | tf_op jit(solution)/shard_map/reduce_scatter | solution.py:31
  524.5 5.8 %psum.31 = f32[512]{0:T(512)S(1)} all-reduce(f32[512]{0:T(512)S(1)} %fusion.31), channel_id=1, replica_groups=mesh['fs'=8,'tp'=4] {'tp'}, use_global_device_ids=true, to_apply=%region_9.10 | all-reduce | flops 512 | bytes 4096 | tf_op jit(solution)/shard_map/psum | solution.py:13
  530.2 2.1 fusion.40
  (161 shorter events, 38.1 us)
Async XLA Ops:
  6.5 58.1 %copy-start = (bf16[2,256,256]{2,1,0:T(8,128)(2,1)S(1)}, bf16[2,256,256]{2,1,0:T(8,128)(2,1)}, u32[]{:S(2)}) copy-start(bf16[2,256,256]{2,1,0:T(8,128)(2,1)} %param.22) | copy-start | bytes 786436
  6.5 54.8 %all-gather.9.cloned.1.call-start = ((), (), s32[]{:S(2)}) async-start(), calls=%async_computation.5 | async-start | bytes 2359296 | tf_op jit(solution)/shard_map/all_gather | solution.py:83
  7.3 148.3 %all-gather.11.cloned.1.call-start = ((), (), s32[]{:S(2)}) async-start(), calls=%async_computation.6 | async-start | bytes 2359296 | tf_op jit(solution)/shard_map/all_gather | solution.py:105
  21.3 4.5 copy-start.23
  21.3 4.6 copy-start.13
  21.3 29.4 %all-to-all-start = ((bf16[4,512,512]{1,2,0:T(8,128)(2,1)}), bf16[4,512,512]{1,2,0:T(8,128)(2,1)S(1)}, u32[]{:S(2)}, u32[]{:S(2)}) async-start(bf16[4,512,512]{1,2,0:T(8,128)(2,1)} %stack.4), calls=%async_computation | async-start | bytes 4194304 | tf_op jit(solution)/shard_map/all_to_all | solution.py:20
  25.1 136.6 %all-gather.7.cloned.1.call-start = ((), (), s32[]{:S(2)}) async-start(), calls=%async_computation.4 | async-start | bytes 2359296 | tf_op jit(solution)/shard_map/all_gather | solution.py:82
  25.8 172.9 %reduce-scatter.3.cloned.1.call-start = ((), (), s32[]{:S(2)}) async-start(), calls=%async_computation.7 | async-start | bytes 2621440 | tf_op jit(solution)/shard_map/reduce_scatter | solution.py:31
  50.7 13.5 %copy-start.3 = (bf16[4,512,512]{1,2,0:T(8,128)(2,1)}, bf16[4,512,512]{1,2,0:T(8,128)(2,1)S(1)}, u32[]{:S(2)}) copy-start(bf16[4,512,512]{1,2,0:T(8,128)(2,1)S(1)} %all-to-all-done) | copy-start | bytes 6291460
  64.7 1.8 copy-start.27
  140.8 5.2 copy-start.12
  140.8 5.2 copy-start.14
  140.8 5.2 copy-start.15
  140.8 5.2 copy-start.18
  140.8 5.2 copy-start.9
  140.8 6.0 %copy-start.10 = (f32[3,512]{1,0:T(4,128)S(1)}, f32[3,512]{1,0:T(4,128)}, u32[]{:S(2)}) copy-start(f32[3,512]{1,0:T(4,128)} %slice.305) | copy-start | bytes 18436
  140.8 6.0 %copy-start.11 = (f32[3,512]{1,0:T(4,128)S(1)}, f32[3,512]{1,0:T(4,128)}, u32[]{:S(2)}) copy-start(f32[3,512]{1,0:T(4,128)} %slice.322) | copy-start | bytes 18436
  140.8 6.1 %copy-start.22 = (f32[1,512]{1,0:T(1,128)S(1)}, f32[1,512]{1,0:T(1,128)}, u32[]{:S(2)}) copy-start(f32[1,512]{1,0:T(1,128)} %slice.355) | copy-start | bytes 6148
  140.8 6.1 %copy-start.8 = (f32[7,512]{1,0:T(8,128)S(1)}, f32[7,512]{1,0:T(8,128)}, u32[]{:S(2)}) copy-start(f32[7,512]{1,0:T(8,128)} %slice.324) | copy-start | bytes 43012
  140.8 6.1 %copy-start.21 = (f32[1,512]{1,0:T(1,128)S(1)}, f32[1,512]{1,0:T(1,128)}, u32[]{:S(2)}) copy-start(f32[1,512]{1,0:T(1,128)} %slice.354) | copy-start | bytes 6148
  140.9 6.2 %copy-start.7 = (f32[15,512]{1,0:T(8,128)S(1)}, f32[15,512]{1,0:T(8,128)}, u32[]{:S(2)}) copy-start(f32[15,512]{1,0:T(8,128)} %slice.293) | copy-start | bytes 92164
  140.9 7.7 %copy-start.6 = (f32[31,512]{1,0:T(8,128)S(1)}, f32[31,512]{1,0:T(8,128)}, u32[]{:S(2)}) copy-start(f32[31,512]{1,0:T(8,128)} %slice.287) | copy-start | bytes 190468
  145.4 6.6 %copy-start.4 = (f32[127,512]{1,0:T(8,128)S(1)}, f32[127,512]{1,0:T(8,128)}, u32[]{:S(2)}) copy-start(f32[127,512]{1,0:T(8,128)} %slice.275) | copy-start | bytes 780292
  145.4 6.6 %copy-start.5 = (f32[127,512]{1,0:T(8,128)S(1)}, f32[127,512]{1,0:T(8,128)}, u32[]{:S(2)}) copy-start(f32[127,512]{1,0:T(8,128)} %slice.332) | copy-start | bytes 780292
  147.0 5.1 copy-start.20
  152.3 3.0 copy-start.19
  168.8 1.9 copy-start.24
  168.8 2.0 copy-start.25
  168.8 37.1 %copy-start.2 = (bf16[512,512]{1,0:T(8,128)(2,1)S(1)}, bf16[512,512]{1,0:T(8,128)(2,1)}, u32[]{:S(2)}) copy-start(bf16[512,512]{1,0:T(8,128)(2,1)} %param.17) | copy-start | bytes 1572868
  168.8 124.2 %all-gather.15.cloned.1.call-start = ((), (), s32[]{:S(2)}) async-start(), calls=%async_computation.9 | async-start | bytes 6488064 | tf_op jit(solution)/shard_map/all_gather | solution.py:116
  169.4 216.2 %all-gather.13.cloned.1.call-start = ((), (), s32[]{:S(2)}) async-start(), calls=%async_computation.8 | async-start | bytes 6488064 | tf_op jit(solution)/shard_map/all_gather | solution.py:115
  170.0 309.0 %all-gather.17.cloned.1.call-start = ((), (), s32[]{:S(2)}) async-start(), calls=%async_computation.10 | async-start | bytes 6488064 | tf_op jit(solution)/shard_map/all_gather | solution.py:124
  213.4 5.2 copy-start.16
  213.5 5.2 copy-start.17
  215.0 29.2 %all-to-all-start.1 = ((bf16[4,512,512]{1,2,0:T(8,128)(2,1)}), bf16[4,512,512]{1,2,0:T(8,128)(2,1)S(1)}, u32[]{:S(2)}, u32[]{:S(2)}) async-start(bf16[4,512,512]{1,2,0:T(8,128)(2,1)} %stack.5), calls=%async_computation.2 | async-start | bytes 4194304 | tf_op jit(solution)/shard_map/all_to_all | solution.py:20
  218.6 304.7 %reduce-scatter.5.cloned.1.call-start = ((), (), s32[]{:S(2)}) async-start(), calls=%async_computation.11 | async-start | bytes 2621440 | tf_op jit(solution)/shard_map/reduce_scatter | solution.py:31
  479.0 14.7 %copy-start.26 = (bf16[512]{0:T(512)(128)(2,1)S(1)}, bf16[512]{0:T(512)(128)(2,1)}, u32[]{:S(2)}) copy-start(bf16[512]{0:T(512)(128)(2,1)} %param.33) | copy-start | bytes 3076
  479.0 53.3 %copy-start.1 = (bf16[2,256,256]{2,1,0:T(8,128)(2,1)S(1)}, bf16[2,256,256]{2,1,0:T(8,128)(2,1)}, u32[]{:S(2)}) copy-start(bf16[2,256,256]{2,1,0:T(8,128)(2,1)} %param.22) | copy-start | bytes 786436
Sparse Core Ops, SparseCore 0:
  9.5 51.7 all-gather.8
  63.3 48.8 all-gather.10
  114.4 47.2 all-gather.6
  169.0 29.7 reduce-scatter.2
  200.7 92.2 all-gather.14
  295.1 90.4 all-gather.12
  387.7 91.2 all-gather.16
  493.9 29.3 reduce-scatter.4
